TPU v7x, 512 devices: a whole 4x4x16 slice. The times are simulated.
512 devices in a mesh: sp: 32 (over z, core), tp: 16 (over y, x).
Axes of the slice: x: 4, y: 4, z: 16, core: 2. Of those that a mesh axis runs over, the one named last changes fastest.
Arguments:
- moe_input: bfloat16 [6144, 2048], P('sp'), may hold values from -6 to 6
- out_grad: bfloat16 [6144, 2048], P('sp'), may hold values from -6 to 6
- route_ids: int32 [6144, 2], P('sp'), may hold values from 0 to 31, all different within a row; in each aligned block of 192 rows (0 to 191, 192 to 383, ...) at most 18 rows name the same one
- route_weights: float32 [6144, 2], P('sp'), may hold values from 0.2 to 2
- expert_gate: bfloat16 [32, 2048, 2048], P('sp', None, 'tp'), may hold values from -0.125 to 0.125
- expert_up: bfloat16 [32, 2048, 2048], P('sp', None, 'tp'), may hold values from -0.125 to 0.125
- expert_down: bfloat16 [32, 2048, 2048], P('sp', 'tp'), may hold values from -0.125 to 0.125
- proj_weight: bfloat16 [1024, 2048], P(None, 'tp'), may hold values from -0.1875 to 0.1875
- glu_value: bfloat16 [1024, 6144], P('tp', 'sp'), may hold values from -6 to 6
- glu_gate: bfloat16 [1024, 6144], P('tp', 'sp'), may hold values from -8 to 8
- conv_taps: float32 [1024, 31], P('tp'), may hold values from -1 to 1
- norm_input: bfloat16 [1024, 6144], P('tp', 'sp'), may hold values from -6 to 6
- norm_gain: float32 [1024], replicated, may hold values from 0.1 to 1.9
Outputs:
- grad_gate: bfloat16 [32, 2048, 2048], P('sp', None, 'tp')
- grad_up: bfloat16 [32, 2048, 2048], P('sp', None, 'tp')
- grad_down: bfloat16 [32, 2048, 2048], P('sp', 'tp')
- grad_proj: float32 [1024, 2048], P('sp', 'tp')
- grad_value: bfloat16 [1024, 6144], P('tp', 'sp')
- grad_glu_gate: bfloat16 [1024, 6144], P('tp', 'sp')
Inputs may be any that keep to these rules, and one draw needn't show every extreme that they name: `route_ids`: within the rows of one device, the 2 ids of a position differ and no expert is named by more than 18 pairs; some expert is named by exactly 18.
All inputs are finite; a program needn't handle non-finite values.
Results may differ from a plain program's by a relative error of at most 0.025.
Values may be sent and summed in bfloat16 or wider, within the bound.
No kernel may reach another device: no remote copies, remote signals or barrier semaphores. Data moves between devices by JAX's collectives and lax.ppermute only.
A program may use at most 64 MiB of HBM per device.

v0:
```python
import jax
import jax.numpy as jnp
from jax import lax
from jax.sharding import Mesh
from jax.sharding import PartitionSpec as P

TP = ("tp_0", "tp_1")


norm_eps = 1e-05


def sent_together(arrays, axis, split_dim, concat_dim, along):
    ends, at = ([], 0)
    for a in arrays[:-1]:
        at += a.shape[along]
        ends.append(at)
    both = jnp.concatenate(arrays, axis=along)
    return tuple(
        jnp.split(
            lax.all_to_all(both, axis, split_axis=split_dim, concat_axis=concat_dim, tiled=True),
            ends,
            axis=along,
        )
    )


def sent_together_2(arrays, axis, dim, along):
    ends, at = ([], 0)
    for a in arrays[:-1]:
        at += a.shape[along]
        ends.append(at)
    both = jnp.concatenate(arrays, axis=along)
    return tuple(jnp.split(lax.all_gather(both, axis, axis=dim, tiled=True), ends, axis=along))


def in_blocks(shard, dim, length):
    before, after = (shard.shape[:dim], shard.shape[dim + 1 :])
    return jnp.moveaxis(shard.reshape(*before, length, -1, *after), dim, 0)


def sum_at_owner(shard, axis, dim):
    length = lax.axis_size(axis)
    blocks = lax.all_to_all(in_blocks(shard, dim, length), axis, 0, 0, tiled=True)
    return jnp.sum(blocks.astype(jnp.float32), axis=0)


def from_everyone(shard, axis):
    length = lax.axis_size(axis)
    return lax.all_to_all(
        jnp.broadcast_to(shard[None], (length, *shard.shape)), axis, 0, 0, tiled=True
    )


def laid_out(blocks, dim):
    blocks = jnp.moveaxis(blocks, 0, dim)
    shape = blocks.shape
    return blocks.reshape(*shape[:dim], shape[dim] * shape[dim + 1], *shape[dim + 2 :])


def gather_directly(shard, axis, dim):
    blocks = from_everyone(shard, axis)
    return laid_out(blocks, dim)


def over_axes(shard, axes):
    for axis in axes:
        shard = lax.psum(shard, axis)
    return shard


def shifted(shard, axis, by):
    length = lax.axis_size(axis)
    pairs = [(i, i + by) for i in range(length) if 0 <= i + by < length]
    return lax.ppermute(shard, axis, pairs)


def silu_grad(pre):
    sigmoid_pre = jax.nn.sigmoid(pre)
    return sigmoid_pre * (1.0 + pre * (1.0 - sigmoid_pre))


def slot_table(route_ids, route_weights, experts, capacity):
    tok_rows, top_count = route_ids.shape
    flat_ids = route_ids.reshape(-1)
    onehot = (flat_ids[:, None] == jnp.arange(experts, dtype=jnp.int32)[None, :]).astype(jnp.int32)
    before = jnp.cumsum(onehot, axis=0) - onehot
    slot_index = jnp.sum(before * onehot, axis=1)
    target = flat_ids * capacity + slot_index
    buffer_rows = jnp.arange(experts * capacity, dtype=jnp.int32)
    matches = (buffer_rows[:, None] == target[None, :]).reshape(
        experts * capacity, tok_rows, top_count
    )
    placing = jnp.sum(matches.astype(jnp.float32), axis=2).astype(jnp.bfloat16)
    slot_scale = jnp.sum(jnp.where(matches, route_weights[None, :, :], 0.0), axis=(1, 2))
    return (placing, slot_scale)


def body(
    moe_input,
    out_grad,
    route_ids,
    route_weights,
    expert_gate,
    expert_up,
    expert_down,
    proj_weight,
    glu_value,
    glu_gate,
    conv_taps,
    norm_input,
    norm_gain,
):
    groups = lax.axis_size("sp")
    lane_count = lax.axis_size(TP)
    lane_index = lax.axis_index(TP)
    tok_rows, model_width = moe_input.shape
    top_count = route_ids.shape[1]
    capacity = tok_rows * top_count * 3 // (2 * groups)
    part_width = model_width // lane_count
    placing, slot_scale = slot_table(route_ids, route_weights, groups, capacity)
    own_grad = lax.dynamic_slice_in_dim(out_grad, lane_index * part_width, part_width, 1)
    own_input = lax.dynamic_slice_in_dim(moe_input, lane_index * part_width, part_width, 1)
    sent_rows = jnp.dot(placing, own_input, preferred_element_type=jnp.float32).astype(jnp.bfloat16)
    sent_grad = (
        jnp.dot(placing, own_grad, preferred_element_type=jnp.float32) * slot_scale[:, None]
    ).astype(jnp.bfloat16)
    part_rows, part_grad = sent_together(
        (
            sent_rows.reshape(groups, capacity, part_width),
            sent_grad.reshape(groups, capacity, part_width),
        ),
        "sp",
        0,
        0,
        1,
    )
    arrived_rows, arrived_grad = sent_together_2((part_rows, part_grad), TP, 2, 0)
    token_rows = arrived_rows.reshape(-1, model_width)
    grad_rows = arrived_grad.reshape(-1, model_width)
    w_gate = expert_gate[0]
    w_up = expert_up[0]
    w_down = expert_down[0]
    gate_pre = jnp.dot(token_rows, w_gate, preferred_element_type=jnp.float32)
    up_pre = jnp.dot(token_rows, w_up, preferred_element_type=jnp.float32)
    gate_act = jax.nn.silu(gate_pre)
    hidden = (gate_act * up_pre).astype(jnp.bfloat16)
    down_grad = lax.dot_general(
        hidden, grad_rows, (((0,), (0,)), ((), ())), preferred_element_type=jnp.float32
    ).astype(jnp.bfloat16)
    grad_hidden = lax.dot_general(
        grad_rows, w_down, (((1,), (1,)), ((), ())), preferred_element_type=jnp.float32
    )
    gate_grad = (grad_hidden * up_pre * silu_grad(gate_pre)).astype(jnp.bfloat16)
    up_grad = (grad_hidden * gate_act).astype(jnp.bfloat16)
    gate_wgrad = lax.dot_general(
        token_rows, gate_grad, (((0,), (0,)), ((), ())), preferred_element_type=jnp.float32
    ).astype(jnp.bfloat16)
    up_wgrad = lax.dot_general(
        token_rows, up_grad, (((0,), (0,)), ((), ())), preferred_element_type=jnp.float32
    ).astype(jnp.bfloat16)
    input_grad = lax.dot_general(
        gate_grad, w_gate, (((1,), (1,)), ((), ())), preferred_element_type=jnp.float32
    )
    input_grad = input_grad + lax.dot_general(
        up_grad, w_up, (((1,), (1,)), ((), ())), preferred_element_type=jnp.float32
    )
    summed_grad = sum_at_owner(input_grad.astype(jnp.bfloat16), TP, 1).astype(jnp.bfloat16)
    returned = lax.all_to_all(
        summed_grad.reshape(groups, capacity, part_width),
        "sp",
        split_axis=0,
        concat_axis=0,
        tiled=True,
    )
    moe_grad = lax.dot_general(
        placing,
        returned.reshape(-1, part_width),
        (((0,), (0,)), ((), ())),
        preferred_element_type=jnp.float32,
    )
    mix_grad = (own_grad.astype(jnp.float32) + moe_grad).astype(jnp.bfloat16)
    channel_part = norm_input.shape[0]
    conv_values = gather_directly(norm_input, TP, 0).astype(jnp.float32)
    channels = conv_values.shape[0]
    centred = conv_values - jnp.mean(conv_values, axis=0, keepdims=True)
    inv_scale = lax.rsqrt(jnp.mean(centred * centred, axis=0, keepdims=True) + norm_eps)
    normed = centred * inv_scale
    scaled = normed * norm_gain[:, None]
    act = jax.nn.silu(scaled).astype(jnp.bfloat16)
    grad_proj = sum_at_owner(
        jnp.dot(act, mix_grad, preferred_element_type=jnp.float32).astype(jnp.bfloat16), "sp", 0
    )
    act_partial = lax.dot_general(
        proj_weight, mix_grad, (((1,), (1,)), ((), ())), preferred_element_type=jnp.float32
    )
    grad_act = sum_at_owner(act_partial.astype(jnp.bfloat16), TP, 0)
    normed_own = lax.dynamic_slice_in_dim(normed, lane_index * channel_part, channel_part, 0)
    scaled_own = lax.dynamic_slice_in_dim(scaled, lane_index * channel_part, channel_part, 0)
    gain_own = lax.dynamic_slice_in_dim(norm_gain, lane_index * channel_part, channel_part, 0)
    grad_normed = grad_act * silu_grad(scaled_own) * gain_own[:, None]
    sum_grad, sum_cross = (
        over_axes(jnp.sum(grad_normed, axis=0), TP),
        over_axes(jnp.sum(grad_normed * normed_own, axis=0), TP),
    )
    grad_conv = inv_scale * (
        grad_normed - sum_grad[None, :] / channels - normed_own * (sum_cross[None, :] / channels)
    )
    taps_count = conv_taps.shape[1]
    reach_back = taps_count - 1
    ahead_rows = shifted(grad_conv[:, :reach_back], "sp", -1)
    extended = jnp.concatenate([grad_conv, ahead_rows], axis=1)
    grad_glu = jnp.zeros_like(grad_conv)
    for tap_index in range(taps_count):
        grad_glu = (
            grad_glu
            + conv_taps[:, tap_index : tap_index + 1]
            * extended[:, reach_back - tap_index : reach_back - tap_index + tok_rows]
        )
    sigmoid_gate = jax.nn.sigmoid(glu_gate.astype(jnp.float32))
    grad_value = (grad_glu * sigmoid_gate).astype(jnp.bfloat16)
    grad_glu_gate = (
        grad_glu * glu_value.astype(jnp.float32) * sigmoid_gate * (1.0 - sigmoid_gate)
    ).astype(jnp.bfloat16)
    return (gate_wgrad[None], up_wgrad[None], down_grad[None], grad_proj, grad_value, grad_glu_gate)


def solution(mesh):
    finer = Mesh(mesh.devices.reshape(mesh.shape["sp"], 4, 4), ("sp", "tp_0", "tp_1"))
    return jax.shard_map(
        body,
        mesh=finer,
        in_specs=(
            P("sp", None),
            P("sp", None),
            P("sp", None),
            P("sp", None),
            P("sp", None, TP),
            P("sp", None, TP),
            P("sp", TP, None),
            P(None, TP),
            P(TP, "sp"),
            P(TP, "sp"),
            P(TP, None),
            P(TP, "sp"),
            P(),
        ),
        out_specs=(
            P("sp", None, TP),
            P("sp", None, TP),
            P("sp", TP, None),
            P("sp", TP),
            P(TP, "sp"),
            P(TP, "sp"),
        ),
        check_vma=False,
    )
```

profile of v0, /device:TPU:1, one launch (start us, length us, event | category | flops | bytes accessed | tf_op | source)
XLA Modules:
  0.0 290.6 jit_solution(6470165151364125645)
XLA Ops:
  7.2 0.9 copy.44
  8.4 0.9 reduce-window.6
  9.9 0.7 multiply_add_fusion
  10.6 0.9 convert_reduce_fusion.1
  11.5 1.1 fusion.5
  13.1 41.5 %all_to_all.30 = bf16[32,36,128]{2,1,0:T(8,128)(2,1)S(1)} all-to-all(bf16[32,36,128]{2,1,0:T(8,128)(2,1)S(1)} %pad_maximum_fusion.1), channel_id=1, replica_groups=mesh['sp'=32,'tp_0'=4,'tp_1'=4] {'sp'}, dimensions={0} | all-to-all | bytes 589824 | tf_op jit(solution)/shard_map/all_to_all | solution.py:21
  54.7 0.8 pad_maximum_fusion
  55.6 0.8 broadcast_in_dim.25
  56.4 6.8 %all-to-all-start.1 = ((bf16[16,64,192]{2,1,0:T(8,128)(2,1)}), bf16[16,64,192]{2,1,0:T(8,128)(2,1)}, u32[]{:S(2)}, u32[]{:S(2)}) async-start(bf16[16,64,192]{2,1,0:T(8,128)(2,1)} %broadcast_in_dim.25), calls=%async_computation.1 | async-start | bytes 1048576 | tf_op jit(solution)/shard_map/all_to_all | solution.py:50
  63.2 64.7 %all-gather.2.cloned.1.call-done = bf16[64,18,2048]{2,1,0:T(8,128)(2,1)} async-done(((bf16[64,18,128]{2,1,0:T(8,128)(2,1)}), bf16[64,18,2048]{2,1,0:T(8,128)(2,1)}) %all-gather.2.cloned.1.call-update) | async-done | bytes 4718608 | tf_op jit(solution)/shard_map/all_gather | solution.py:34
  128.0 6.6 %fusion.123 = (bf16[32,18,2048]{2,1,0:T(8,128)(2,1)}, bf16[32,18,2048]{2,1,0:T(8,128)(2,1)}) fusion(bf16[64,18,2048]{2,1,0:T(8,128)(2,1)} %all-gather.2.cloned.1.call-done), kind=kLoop, calls=%fused_computation.232 | loop fusion | bytes 9437184 | tf_op jit(solution)/shard_map/split | solution.py:34
  134.6 2.9 %reshape.106 = bf16[576,2048]{1,0:T(8,128)(2,1)S(1)} reshape(bf16[32,18,2048]{2,1,0:T(8,128)(2,1)} %get-tuple-element.18) | data formatting | bytes 4718592 | tf_op jit(solution)/shard_map/reshape | solution.py:139
  137.5 2.6 fusion.10
  140.1 1.5 fusion.13
  141.6 4.3 %reshape.107 = bf16[576,2048]{1,0:T(8,128)(2,1)} reshape(bf16[32,18,2048]{2,1,0:T(8,128)(2,1)} %get-tuple-element.17) | data formatting | bytes 4718592 | tf_op jit(solution)/shard_map/reshape | solution.py:140
  145.9 2.8 multiply_convert_fusion.3
  148.7 0.8 fusion.8
  149.9 0.8 fusion.3
  150.6 2.1 copy.54
  152.7 4.8 %all-to-all-start.2 = ((bf16[16,576,128]{2,1,0:T(8,128)(2,1)}), bf16[16,576,128]{2,1,0:T(8,128)(2,1)}, u32[]{:S(2)}, u32[]{:S(2)}) async-start(bf16[16,576,128]{2,1,0:T(8,128)(2,1)} %bitcast.138), calls=%async_computation.2 | async-start | bytes 4718592 | tf_op jit(solution)/shard_map/all_to_all | solution.py:44
  159.5 1.2 convert_reduce_fusion.2
  160.7 1.2 multiply_reduce_fusion
  161.9 26.0 %all-to-all-done.2 = bf16[16,576,128]{2,1,0:T(8,128)(2,1)} async-done(((bf16[16,576,128]{2,1,0:T(8,128)(2,1)}), bf16[16,576,128]{2,1,0:T(8,128)(2,1)}, u32[]{:S(2)}, u32[]{:S(2)}) %all-to-all-start.2) | async-done | bytes 2359328 | tf_op jit(solution)/shard_map/all_to_all | solution.py:44
  188.0 2.0 reduce_sum.101
  190.0 0.7 reshape.109
  190.7 16.8 %all-to-all-start.3 = ((bf16[32,18,128]{2,1,0:T(8,128)(2,1)}), bf16[32,18,128]{2,1,0:T(8,128)(2,1)}, u32[]{:S(2)}, u32[]{:S(2)}) async-start(bf16[32,18,128]{2,1,0:T(8,128)(2,1)} %reshape.109), calls=%async_computation.3 | async-start | bytes 393216 | tf_op jit(solution)/shard_map/all_to_all | solution.py:169
  208.1 2.7 fusion.7
  210.8 2.5 fusion.2
  213.3 13.1 %all-to-all-done.3 = bf16[32,18,128]{2,1,0:T(8,128)(2,1)} async-done(((bf16[32,18,128]{2,1,0:T(8,128)(2,1)}), bf16[32,18,128]{2,1,0:T(8,128)(2,1)}, u32[]{:S(2)}, u32[]{:S(2)}) %all-to-all-start.3) | async-done | bytes 147488 | tf_op jit(solution)/shard_map/all_to_all | solution.py:169
  226.4 1.0 reshape.110
  227.4 1.0 fusion.6
  229.0 1.2 fusion.4
  230.2 1.0 copy.49
  231.2 4.4 %all-to-all-start.5 = ((bf16[16,64,192]{2,1,0:T(8,128)(2,1)}), bf16[16,64,192]{2,1,0:T(8,128)(2,1)}, u32[]{:S(2)}, u32[]{:S(2)}) async-start(bf16[16,64,192]{2,1,0:T(8,128)(2,1)} %bitcast.139), calls=%async_computation.5 | async-start | bytes 1048576 | tf_op jit(solution)/shard_map/all_to_all | solution.py:44
  235.7 2.7 fusion
  238.4 1.1 convolution_convert_fusion.4
  239.5 6.2 %all-to-all-done.5 = bf16[16,64,192]{2,1,0:T(8,128)(2,1)} async-done(((bf16[16,64,192]{2,1,0:T(8,128)(2,1)}), bf16[16,64,192]{2,1,0:T(8,128)(2,1)}, u32[]{:S(2)}, u32[]{:S(2)}) %all-to-all-start.5) | async-done | bytes 393248 | tf_op jit(solution)/shard_map/all_to_all | solution.py:44
  245.7 5.8 %all-to-all-start.4 = ((bf16[32,32,128]{2,1,0:T(8,128)(2,1)}), bf16[32,32,128]{2,1,0:T(8,128)(2,1)S(1)}, u32[]{:S(2)}, u32[]{:S(2)}) async-start(bf16[32,32,128]{2,1,0:T(8,128)(2,1)} %bitcast.140), calls=%async_computation.4 | async-start | bytes 524288 | tf_op jit(solution)/shard_map/all_to_all | solution.py:44
  251.5 1.1 convert_reduce_fusion
  252.6 2.2 fusion.121
  254.8 7.8 %all-reduce.1 = (f32[192]{0:T(256)}, f32[192]{0:T(256)}) all-reduce(f32[192]{0:T(256)} %get-tuple-element.7, f32[192]{0:T(256)} %get-tuple-element.6), channel_id=1, replica_groups=mesh['sp'=32,'tp_0'=4,'tp_1'=4] {'tp_0'}, use_global_device_ids=true, to_apply=%region_14.15 | all-reduce | flops 384 | bytes 3072 | tf_op jit(solution)/shard_map/psum | solution.py:68
  262.6 7.6 %all-reduce = (f32[192]{0:T(256)}, f32[192]{0:T(256)}) all-reduce(f32[192]{0:T(256)} %get-tuple-element.12, f32[192]{0:T(256)} %get-tuple-element.13), channel_id=1, replica_groups=mesh['sp'=32,'tp_0'=4,'tp_1'=4] {'tp_1'}, use_global_device_ids=true, to_apply=%region_15.16 | all-reduce | flops 384 | bytes 3072 | tf_op jit(solution)/shard_map/psum | solution.py:68
  270.1 0.7 broadcast_multiply_fusion.1
  270.8 0.9 subtract_multiply_fusion
  272.1 5.4 %collective-permute-start = (f32[64,30]{1,0:T(8,128)S(1)}, f32[64,30]{1,0:T(8,128)S(1)}, u32[]{:S(2)}, u32[]{:S(2)}) collective-permute-start(f32[64,30]{1,0:T(8,128)S(1)} %slice.257), channel_id=1, source_target_pairs={{16,0},{32,16},{48,32},{64,48},{80,64},{96,80},{112,96},{128,112},... | collective-permute-start | bytes 23048 | tf_op jit(solution)/shard_map/ppermute | solution.py:75
  277.5 1.7 fusion.1
  279.2 1.2 collective-permute-done
  280.7 1.8 multiply_convert_fusion.6
  (121 shorter events, 6.4 us)
Async XLA Ops:
  7.2 5.5 %copy-start = (bf16[192,2048]{1,0:T(8,128)(2,1)S(1)}, bf16[192,2048]{1,0:T(8,128)(2,1)}, u32[]{:S(2)}) copy-start(bf16[192,2048]{1,0:T(8,128)(2,1)} %param.13) | copy-start | bytes 2359300
  7.2 120.8 %all-gather.2.cloned.1.call-start = ((), (), s32[]{:S(2)}) async-start(), calls=%async_computation.6 | async-start | bytes 6684672 | tf_op jit(solution)/shard_map/all_gather | solution.py:34
  11.5 44.0 %copy-start.12 = (bf16[64,192]{1,0:T(8,128)(2,1)S(1)}, bf16[64,192]{1,0:T(8,128)(2,1)}, u32[]{:S(2)}) copy-start(bf16[64,192]{1,0:T(8,128)(2,1)} %param.24) | copy-start | bytes 73732
  56.4 96.3 %all-to-all-start.1 = ((bf16[16,64,192]{2,1,0:T(8,128)(2,1)}), bf16[16,64,192]{2,1,0:T(8,128)(2,1)}, u32[]{:S(2)}, u32[]{:S(2)}) async-start(bf16[16,64,192]{2,1,0:T(8,128)(2,1)} %broadcast_in_dim.25), calls=%async_computation.1 | async-start | bytes 1048576 | tf_op jit(solution)/shard_map/all_to_all | solution.py:50
  145.9 2.8 copy-start.2
  152.7 4.9 %copy-start.16 = (f32[1024]{0:T(1024)S(1)}, f32[1024]{0:T(1024)}, u32[]{:S(2)}) copy-start(f32[1024]{0:T(1024)} %param.25) | copy-start | bytes 12292
  152.7 5.5 %copy-start.14 = (f32[64,31]{0,1:T(8,128)S(1)}, f32[64,31]{0,1:T(8,128)}, u32[]{:S(2)}) copy-start(f32[64,31]{0,1:T(8,128)} %param.23) | copy-start | bytes 23812
  152.7 35.3 %all-to-all-start.2 = ((bf16[16,576,128]{2,1,0:T(8,128)(2,1)}), bf16[16,576,128]{2,1,0:T(8,128)(2,1)}, u32[]{:S(2)}, u32[]{:S(2)}) async-start(bf16[16,576,128]{2,1,0:T(8,128)(2,1)} %bitcast.138), calls=%async_computation.2 | async-start | bytes 4718592 | tf_op jit(solution)/shard_map/all_to_all | solution.py:44
  190.7 35.7 %all-to-all-start.3 = ((bf16[32,18,128]{2,1,0:T(8,128)(2,1)}), bf16[32,18,128]{2,1,0:T(8,128)(2,1)}, u32[]{:S(2)}, u32[]{:S(2)}) async-start(bf16[32,18,128]{2,1,0:T(8,128)(2,1)} %reshape.109), calls=%async_computation.3 | async-start | bytes 393216 | tf_op jit(solution)/shard_map/all_to_all | solution.py:169
  207.6 3.2 %copy-start.1 = (bf16[576,2048]{1,0:T(8,128)(2,1)S(1)}, bf16[576,2048]{1,0:T(8,128)(2,1)}, u32[]{:S(2)}) copy-start(bf16[576,2048]{1,0:T(8,128)(2,1)} %reshape.107) | copy-start | bytes 7077892
  231.2 14.5 %all-to-all-start.5 = ((bf16[16,64,192]{2,1,0:T(8,128)(2,1)}), bf16[16,64,192]{2,1,0:T(8,128)(2,1)}, u32[]{:S(2)}, u32[]{:S(2)}) async-start(bf16[16,64,192]{2,1,0:T(8,128)(2,1)} %bitcast.139), calls=%async_computation.5 | async-start | bytes 1048576 | tf_op jit(solution)/shard_map/all_to_all | solution.py:44
  235.7 2.7 copy-start.5
  238.4 39.1 %copy-start.7 = (bf16[576,128]{1,0:T(8,128)(2,1)S(1)}, bf16[576,128]{1,0:T(8,128)(2,1)}, u32[]{:S(2)}) copy-start(bf16[576,128]{1,0:T(8,128)(2,1)} %copy-done.6) | copy-start | bytes 442372
  245.7 37.4 %all-to-all-start.4 = ((bf16[32,32,128]{2,1,0:T(8,128)(2,1)}), bf16[32,32,128]{2,1,0:T(8,128)(2,1)S(1)}, u32[]{:S(2)}, u32[]{:S(2)}) async-start(bf16[32,32,128]{2,1,0:T(8,128)(2,1)} %bitcast.140), calls=%async_computation.4 | async-start | bytes 524288 | tf_op jit(solution)/shard_map/all_to_all | solution.py:44
  271.7 8.6 %copy-start.11 = (bf16[64,192]{1,0:T(8,128)(2,1)S(1)}, bf16[64,192]{1,0:T(8,128)(2,1)}, u32[]{:S(2)}) copy-start(bf16[64,192]{1,0:T(8,128)(2,1)} %param.22) | copy-start | bytes 73732
  271.7 8.6 %copy-start.13 = (bf16[64,192]{1,0:T(8,128)(2,1)S(1)}, bf16[64,192]{1,0:T(8,128)(2,1)}, u32[]{:S(2)}) copy-start(bf16[64,192]{1,0:T(8,128)(2,1)} %param.21) | copy-start | bytes 73732
  271.8 8.6 %copy-start.17 = (f32[64]{0:T(128)S(1)}, f32[64]{0:T(128)}, u32[]{:S(2)}) copy-start(f32[64]{0:T(128)} %get-tuple-element.44) | copy-start | bytes 772
  271.8 8.6 %copy-start.18 = (f32[64]{0:T(128)S(1)}, f32[64]{0:T(128)}, u32[]{:S(2)}) copy-start(f32[64]{0:T(128)} %get-tuple-element.45) | copy-start | bytes 772
  271.8 8.6 %copy-start.19 = (f32[64]{0:T(128)S(1)}, f32[64]{0:T(128)}, u32[]{:S(2)}) copy-start(f32[64]{0:T(128)} %get-tuple-element.46) | copy-start | bytes 772
  271.8 8.6 %copy-start.20 = (f32[64]{0:T(128)S(1)}, f32[64]{0:T(128)}, u32[]{:S(2)}) copy-start(f32[64]{0:T(128)} %get-tuple-element.47) | copy-start | bytes 772
  271.8 8.6 %copy-start.21 = (f32[64]{0:T(128)S(1)}, f32[64]{0:T(128)}, u32[]{:S(2)}) copy-start(f32[64]{0:T(128)} %get-tuple-element.48) | copy-start | bytes 772
  271.8 8.6 %copy-start.22 = (f32[64]{0:T(128)S(1)}, f32[64]{0:T(128)}, u32[]{:S(2)}) copy-start(f32[64]{0:T(128)} %get-tuple-element.49) | copy-start | bytes 772
  271.8 8.6 %copy-start.23 = (f32[64]{0:T(128)S(1)}, f32[64]{0:T(128)}, u32[]{:S(2)}) copy-start(f32[64]{0:T(128)} %get-tuple-element.50) | copy-start | bytes 772
  271.8 8.6 %copy-start.24 = (f32[64]{0:T(128)S(1)}, f32[64]{0:T(128)}, u32[]{:S(2)}) copy-start(f32[64]{0:T(128)} %get-tuple-element.51) | copy-start | bytes 772
  271.8 8.6 %copy-start.25 = (f32[64]{0:T(128)S(1)}, f32[64]{0:T(128)}, u32[]{:S(2)}) copy-start(f32[64]{0:T(128)} %get-tuple-element.52) | copy-start | bytes 772
  271.8 8.6 %copy-start.26 = (f32[64]{0:T(128)S(1)}, f32[64]{0:T(128)}, u32[]{:S(2)}) copy-start(f32[64]{0:T(128)} %get-tuple-element.53) | copy-start | bytes 772
  271.9 8.6 %copy-start.27 = (f32[64]{0:T(128)S(1)}, f32[64]{0:T(128)}, u32[]{:S(2)}) copy-start(f32[64]{0:T(128)} %get-tuple-element.54) | copy-start | bytes 772
  271.9 8.6 %copy-start.28 = (f32[64]{0:T(128)S(1)}, f32[64]{0:T(128)}, u32[]{:S(2)}) copy-start(f32[64]{0:T(128)} %get-tuple-element.55) | copy-start | bytes 772
  271.9 8.6 %copy-start.29 = (f32[64]{0:T(128)S(1)}, f32[64]{0:T(128)}, u32[]{:S(2)}) copy-start(f32[64]{0:T(128)} %get-tuple-element.25) | copy-start | bytes 772
  271.9 8.6 %copy-start.30 = (f32[64]{0:T(128)S(1)}, f32[64]{0:T(128)}, u32[]{:S(2)}) copy-start(f32[64]{0:T(128)} %get-tuple-element.26) | copy-start | bytes 772
  271.9 8.6 %copy-start.31 = (f32[64]{0:T(128)S(1)}, f32[64]{0:T(128)}, u32[]{:S(2)}) copy-start(f32[64]{0:T(128)} %get-tuple-element.27) | copy-start | bytes 772
  271.9 8.6 %copy-start.32 = (f32[64]{0:T(128)S(1)}, f32[64]{0:T(128)}, u32[]{:S(2)}) copy-start(f32[64]{0:T(128)} %get-tuple-element.28) | copy-start | bytes 772
  271.9 8.6 %copy-start.33 = (f32[64]{0:T(128)S(1)}, f32[64]{0:T(128)}, u32[]{:S(2)}) copy-start(f32[64]{0:T(128)} %get-tuple-element.29) | copy-start | bytes 772
  271.9 8.6 %copy-start.34 = (f32[64]{0:T(128)S(1)}, f32[64]{0:T(128)}, u32[]{:S(2)}) copy-start(f32[64]{0:T(128)} %get-tuple-element.30) | copy-start | bytes 772
  271.9 8.6 %copy-start.35 = (f32[64]{0:T(128)S(1)}, f32[64]{0:T(128)}, u32[]{:S(2)}) copy-start(f32[64]{0:T(128)} %get-tuple-element.31) | copy-start | bytes 772
  271.9 8.6 %copy-start.36 = (f32[64]{0:T(128)S(1)}, f32[64]{0:T(128)}, u32[]{:S(2)}) copy-start(f32[64]{0:T(128)} %get-tuple-element.32) | copy-start | bytes 772
  272.0 8.6 %copy-start.37 = (f32[64]{0:T(128)S(1)}, f32[64]{0:T(128)}, u32[]{:S(2)}) copy-start(f32[64]{0:T(128)} %get-tuple-element.33) | copy-start | bytes 772
  272.0 8.6 %copy-start.38 = (f32[64]{0:T(128)S(1)}, f32[64]{0:T(128)}, u32[]{:S(2)}) copy-start(f32[64]{0:T(128)} %get-tuple-element.34) | copy-start | bytes 772
  272.0 8.6 %copy-start.39 = (f32[64]{0:T(128)S(1)}, f32[64]{0:T(128)}, u32[]{:S(2)}) copy-start(f32[64]{0:T(128)} %get-tuple-element.35) | copy-start | bytes 772
  272.0 8.6 %copy-start.40 = (f32[64]{0:T(128)S(1)}, f32[64]{0:T(128)}, u32[]{:S(2)}) copy-start(f32[64]{0:T(128)} %get-tuple-element.36) | copy-start | bytes 772
  272.0 8.6 %copy-start.41 = (f32[64]{0:T(128)S(1)}, f32[64]{0:T(128)}, u32[]{:S(2)}) copy-start(f32[64]{0:T(128)} %get-tuple-element.37) | copy-start | bytes 772
  272.0 8.6 %copy-start.42 = (f32[64]{0:T(128)S(1)}, f32[64]{0:T(128)}, u32[]{:S(2)}) copy-start(f32[64]{0:T(128)} %get-tuple-element.38) | copy-start | bytes 772
  272.0 8.6 %copy-start.43 = (f32[64]{0:T(128)S(1)}, f32[64]{0:T(128)}, u32[]{:S(2)}) copy-start(f32[64]{0:T(128)} %get-tuple-element.39) | copy-start | bytes 772
  272.0 8.6 %copy-start.44 = (f32[64]{0:T(128)S(1)}, f32[64]{0:T(128)}, u32[]{:S(2)}) copy-start(f32[64]{0:T(128)} %get-tuple-element.40) | copy-start | bytes 772
  272.0 8.6 %copy-start.45 = (f32[64]{0:T(128)S(1)}, f32[64]{0:T(128)}, u32[]{:S(2)}) copy-start(f32[64]{0:T(128)} %get-tuple-element.41) | copy-start | bytes 772
  272.0 8.6 %copy-start.46 = (f32[64]{0:T(128)S(1)}, f32[64]{0:T(128)}, u32[]{:S(2)}) copy-start(f32[64]{0:T(128)} %get-tuple-element.42) | copy-start | bytes 772
  272.1 8.6 %copy-start.47 = (f32[64]{0:T(128)S(1)}, f32[64]{0:T(128)}, u32[]{:S(2)}) copy-start(f32[64]{0:T(128)} %get-tuple-element.43) | copy-start | bytes 772
  272.1 8.3 %collective-permute-start = (f32[64,30]{1,0:T(8,128)S(1)}, f32[64,30]{1,0:T(8,128)S(1)}, u32[]{:S(2)}, u32[]{:S(2)}) collective-permute-start(f32[64,30]{1,0:T(8,128)S(1)} %slice.257), channel_id=1, source_target_pairs={{16,0},{32,16},{48,32},{64,48},{80,64},{96,80},{112,96},{128,112},... | collective-permute-start | bytes 23048 | tf_op jit(solution)/shard_map/ppermute | solution.py:75
  (7 other events, 9.3 us)
Sparse Core Ops, SparseCore 0:
  55.7 72.2 all-gather.1
where the time goes:
time: 292 us; the launch traced here: 291 us
  waiting for transfers between devices  111 us (38%)
  blocking collectives  56.9 us (19%)
  starting transfers between devices  44.1 us (15%)
  local copies, waits for them, and re-layouts  24.8 us (8%)
  matrix products  20 us (7%)
  other arithmetic  18.6 us (6%)
  between operations  14.9 us (5%)
    all_gather x1, waiting for transfers between devices, sent_together_2(): lax.all_gather(both, axis, axis=dim, tiled=True)  64.7 us
    all_to_all x1, blocking collectives, sent_together(): lax.all_to_all(both, axis, split_axis=split_dim, concat_axis=concat_dim,...  41.5 us
    all_to_all x3, waiting for transfers between devices, sum_at_owner(): lax.all_to_all(in_blocks(shard, dim, length), axis, 0, 0, tiled=True)  32.2 us
    all_to_all x1, starting transfers between devices, body(): lax.all_to_all(summed_grad.reshape(groups, capacity, part_width), 'sp', s...  16.8 us
    psum x2, blocking collectives, over_axes(): shard = lax.psum(shard, axis)  15.4 us
    all_to_all x3, starting transfers between devices, sum_at_owner(): lax.all_to_all(in_blocks(shard, dim, length), axis, 0, 0, tiled=True)  15 us
    all_to_all x1, waiting for transfers between devices, body(): lax.all_to_all(summed_grad.reshape(groups, capacity, part_width), 'sp', s...  13.1 us
    all_to_all x1, starting transfers between devices, from_everyone(): lax.all_to_all(jnp.broadcast_to(shard[None], (length, *shard.shape)), axi...  6.81 us
  transfers between devices with their start and end apart: 7, of which 5 were waited for; matrix products, arithmetic and copies ran while one was open for 16% of the time, Pallas kernels for 0%

commit v1 on v0

v1 whole, which is shorter than its diff:
```python
import jax
import jax.numpy as jnp
from jax import lax
from jax.experimental import pallas as pl
from jax.experimental.pallas import tpu as pltpu
from jax.sharding import Mesh
from jax.sharding import PartitionSpec as P

TP = ("ty", "tx")
SP = ("z", "core")
PLANE = ("core", "ty", "tx")

norm_eps = 1e-05

bf16, f32, i32 = jnp.bfloat16, jnp.float32, jnp.int32


def exchanged(blocks, axis, index_groups=None):
    return lax.all_to_all(blocks, axis, 0, 0, axis_index_groups=index_groups, tiled=True)


def line_groups(ny, nx):
    along_x = [[y * nx + x for x in range(nx)] for y in range(ny)]
    along_y = [[y * nx + x for y in range(ny)] for x in range(nx)]
    count = ny * nx

    def of_core_one(lines):
        return [[count + i for i in line] for line in lines]

    return along_x + of_core_one(along_y), along_y + of_core_one(along_x)


def silu_grad(pre):
    sig = jax.nn.sigmoid(pre)
    return sig * (1.0 + pre * (1.0 - sig))


def contract(a, b, dim_a, dim_b):
    return lax.dot_general(a, b, (((dim_a,), (dim_b,)), ((), ())), preferred_element_type=f32)


def iota(shape, dim):
    return lax.broadcasted_iota(i32, shape, dim)


def whole():
    return pl.BlockSpec(memory_space=pltpu.VMEM)


def scalar():
    return pl.BlockSpec(memory_space=pltpu.SMEM)


def params(mib):
    return pltpu.CompilerParams(vmem_limit_bytes=mib * 1024 * 1024)


def cost(flops, size):
    return pl.CostEstimate(flops=flops, bytes_accessed=size, transcendentals=0)


def one_if(condition):
    return jnp.where(condition, 1.0, 0.0).astype(bf16)


def prep_kernel(lane_ref, ids_ref, scale_ref, input_ref, grad_ref, *outs, capacity, experts):
    del lane_ref
    sent_ref, back_ref, own_ref = outs
    tok = input_ref.shape[0]
    e0, e1 = ids_ref[0:1, :], ids_ref[1:2, :]
    s0, s1 = scale_ref[0:1, :], scale_ref[1:2, :]
    rows = iota((experts, tok), 0)
    hit0, hit1 = rows == e0, rows == e1
    earlier = one_if(iota((tok, tok), 0) < iota((tok, tok), 1))
    before = jnp.dot(one_if(hit0 | hit1), earlier, preferred_element_type=f32)
    slot0 = jnp.sum(jnp.where(hit0, before, 0.0), axis=0, keepdims=True).astype(i32)
    slot1 = jnp.sum(jnp.where(hit1, before, 0.0), axis=0, keepdims=True).astype(i32)
    x = input_ref[...]
    grad = grad_ref[...]
    own_ref[...] = grad
    diagonal = iota((tok, tok), 0) == iota((tok, tok), 1)
    c0 = jnp.sum(jnp.where(diagonal, s0, 0.0), axis=1, keepdims=True)
    c1 = jnp.sum(jnp.where(diagonal, s1, 0.0), axis=1, keepdims=True)
    g = grad.astype(f32)
    g0, g1 = (g * c0).astype(bf16), (g * c1).astype(bf16)
    pitch = sent_ref.shape[0] // experts
    r = iota((sent_ref.shape[0], tok), 0)
    a0, a1 = e0 * pitch + slot0, e1 * pitch + slot1
    half = pitch // 2
    sent = jnp.dot(one_if((r == a0) | (r == a1)), x, preferred_element_type=f32)
    sent = sent + jnp.dot(one_if(r == a0 + half), g0, preferred_element_type=f32)
    sent = sent + jnp.dot(one_if(r == a1 + half), g1, preferred_element_type=f32)
    sent_ref[...] = sent.astype(bf16)
    back_pitch = back_ref.shape[0] // experts
    r = iota((back_ref.shape[0], tok), 0)
    back_ref[...] = one_if((r == e0 * back_pitch + slot0) | (r == e1 * back_pitch + slot1))


def packed(block):
    lanes = 128
    wide = block[:, :lanes]
    rest = block[:, lanes:]
    rows = rest.shape[0] // 2
    return wide, jnp.concatenate([rest[:rows], rest[rows:]], axis=1)


def unpacked(wide, rest):
    lanes = rest.shape[1] // 2
    tail = jnp.concatenate([rest[:, :lanes], rest[:, lanes:]], axis=0)
    return jnp.concatenate([wide, tail], axis=1)


def compact_kernel(part_ref, norm_ref, out_ref, *, capacity, pitch, sources, group):
    copies, _, width = out_ref.shape
    total = sources * capacity
    rows_in, rows_out = group * pitch, group * capacity
    into, outof = iota((rows_out, rows_in), 0), iota((rows_out, rows_in), 1)
    pick_x = one_if(outof == (into // capacity) * pitch + into % capacity)
    pick_g = one_if(outof == (into // capacity) * pitch + into % capacity + pitch // 2)
    for start in range(0, sources // group):
        piece = part_ref[pl.ds(start * rows_in, rows_in), :]
        x = jnp.dot(pick_x, piece, preferred_element_type=f32).astype(bf16)
        g = jnp.dot(pick_g, piece, preferred_element_type=f32).astype(bf16)
        for c in range(copies):
            out_ref[c, pl.ds(start * rows_out, rows_out), :] = x
            out_ref[c, pl.ds(total + start * rows_out, rows_out), :] = g
    wide, rest = packed(norm_ref[...].astype(f32))
    for c in range(copies):
        out_ref[c, pl.ds(2 * total, wide.shape[0]), :] = wide.astype(bf16)
        out_ref[c, pl.ds(2 * total + wide.shape[0], rest.shape[0]), :] = rest.astype(bf16)


def piece_at(core, y, x):
    return jnp.where(core == 0, y, x), jnp.where(core == 0, x, y)


def expert_kernel(core_ref, rows_ref, grads_ref, gate_ref, up_ref, down_ref, *outs):
    back_ref, hidden_ref, both_ref = outs
    core = core_ref[0]
    ny, nx, _, width = rows_ref.shape
    w_both = jnp.concatenate([gate_ref[...], up_ref[...]], axis=1)
    ff = gate_ref.shape[1]

    def features(ref):
        pieces = []
        for y in range(ny):
            for x in range(nx):
                a, b = piece_at(core, y, x)
                pieces.append(ref[a, b])
        return jnp.concatenate(pieces, axis=1)

    pre = jnp.dot(features(rows_ref), w_both, preferred_element_type=f32)
    gate_pre, up_pre = pre[:, :ff], pre[:, ff:]
    d_hidden = contract(features(grads_ref), down_ref[...], 1, 1)
    sig = jax.nn.sigmoid(gate_pre)
    gate_act = gate_pre * sig
    hidden_ref[...] = (gate_act * up_pre).astype(bf16)
    d_gate = d_hidden * up_pre * (sig * (1.0 + gate_pre * (1.0 - sig)))
    d_up = d_hidden * gate_act
    both = jnp.concatenate([d_gate.astype(bf16), d_up.astype(bf16)], axis=1)
    both_ref[...] = both
    back = contract(both, w_both, 1, 1).astype(bf16)
    for j in range(ny * nx):
        back_ref[j] = back[:, j * width : (j + 1) * width]


def weight_kernel(core_ref, rows_ref, grads_ref, hidden_ref, both_ref, *outs):
    del core_ref
    gate_ref, up_ref, down_ref = outs
    ff = hidden_ref.shape[1]
    pair = contract(rows_ref[0, 0], both_ref[...], 0, 0)
    gate_ref[...] = pair[:, :ff].astype(bf16)
    up_ref[...] = pair[:, ff:].astype(bf16)
    down_ref[...] = contract(hidden_ref[...], grads_ref[0, 0], 0, 0).astype(bf16)


def norm_kernel(core_ref, parts_ref, gain_ref, *outs):
    act_ref, slope_ref, cross_ref, stats_ref = outs
    core = core_ref[0]
    ny, nx, height, _ = parts_ref.shape
    part = height * 2 // 3
    blocks = []
    for y in range(ny):
        for x in range(nx):
            a, b = piece_at(core, y, x)
            block = parts_ref[a, b].astype(f32)
            blocks.append(unpacked(block[:part], block[part:]))
    values = jnp.concatenate(blocks, axis=0)
    channels = values.shape[0]
    mean = jnp.sum(values, axis=0, keepdims=True) / channels
    centred = values - mean
    inv = lax.rsqrt(jnp.sum(centred * centred, axis=0, keepdims=True) / channels + norm_eps)
    gain = gain_ref[...]
    normed = centred * inv
    scaled = normed * gain
    sig = jax.nn.sigmoid(scaled)
    act_ref[...] = (scaled * sig).astype(bf16)
    slope = sig * (1.0 + scaled * (1.0 - sig)) * gain
    slope_ref[...] = slope
    cross_ref[...] = slope * normed
    stats_ref[0:1, :] = mean
    stats_ref[1:2, :] = inv


def row_sum_kernel(parts_ref, out_ref, *, capacity, pitch, group):
    count, total, _ = parts_ref.shape
    rows_in, rows_out = group * capacity, group * pitch
    into, outof = iota((rows_out, rows_in), 0), iota((rows_out, rows_in), 1)
    spread = one_if(
        (outof == (into // pitch) * capacity + into % pitch) & (into % pitch < capacity)
    )
    for start in range(0, total // rows_in):
        at = pl.ds(start * rows_in, rows_in)
        acc = parts_ref[0, at, :].astype(f32)
        for j in range(1, count):
            acc = acc + parts_ref[j, at, :].astype(f32)
        moved = jnp.dot(spread, acc.astype(bf16), preferred_element_type=f32)
        out_ref[pl.ds(start * rows_out, rows_out), :] = moved.astype(bf16)


def mix_kernel(core_ref, back_ref, returned_ref, own_ref, proj_ref, act_ref, slope_ref, cross_ref, *outs):
    kept_ref, given_ref, blocks_ref = outs
    core = core_ref[0]
    moe = contract(back_ref[...], returned_ref[...], 0, 0)
    mix = (own_ref[...].astype(f32) + moe).astype(bf16)
    d_act = contract(proj_ref[...], mix, 1, 1)
    lanes = 128

    def as_rows(line):
        rest = line[:, lanes:]
        return [line[:, :lanes], jnp.concatenate([rest, jnp.zeros_like(rest)], axis=1)]

    tail = []
    for ref in (slope_ref, cross_ref):
        line = jnp.sum(ref[...] * d_act, axis=0, keepdims=True)
        high = line.astype(bf16).astype(f32)
        tail += as_rows(high) + as_rows(line - high)
    tail = jnp.concatenate(tail, axis=0).astype(bf16)
    count = blocks_ref.shape[0]
    part = d_act.shape[0] // count
    for j in range(count):
        wide, rest = packed(d_act[j * part : (j + 1) * part])
        blocks_ref[j, pl.ds(0, part), :] = wide.astype(bf16)
        blocks_ref[j, pl.ds(part, part // 2), :] = rest.astype(bf16)
        blocks_ref[j, pl.ds(part * 3 // 2, 8), :] = tail
    grad = jnp.dot(act_ref[...], mix, preferred_element_type=f32)
    size = kept_ref.shape[1]
    for k in range(kept_ref.shape[0]):
        even = grad[2 * k * size : (2 * k + 1) * size]
        odd = grad[(2 * k + 1) * size : (2 * k + 2) * size]
        kept_ref[k] = jnp.where(core == 0, even, odd)
        given_ref[k] = jnp.where(core == 0, odd, even).astype(bf16)


def conv_grad_kernel(blocks_ref, norm_ref, gain_ref, stats_ref, out_ref, head_ref, *, channels):
    count, height, _ = blocks_ref.shape
    acc = blocks_ref[0].astype(f32)
    for j in range(1, count):
        acc = acc + blocks_ref[j].astype(f32)
    part = out_ref.shape[0]
    grad_act = unpacked(acc[:part], acc[part : part * 3 // 2])
    tail = acc[part * 3 // 2 :]

    def line(at):
        rest = tail[at + 1 : at + 2] + tail[at + 3 : at + 4]
        return jnp.concatenate([tail[at : at + 1] + tail[at + 2 : at + 3], rest[:, : rest.shape[1] // 2]], axis=1)

    mean, inv = stats_ref[0:1, :], stats_ref[1:2, :]
    gain = gain_ref[...]
    normed = (norm_ref[...].astype(f32) - mean) * inv
    grad_normed = grad_act * silu_grad(normed * gain) * gain
    out = inv * (grad_normed - line(0) / channels - normed * (line(4) / channels))
    out_ref[...] = out
    head_ref[...] = out[:, : head_ref.shape[1]]


def body(
    moe_input,
    out_grad,
    route_ids,
    route_weights,
    expert_gate,
    expert_up,
    expert_down,
    proj_weight,
    glu_value,
    glu_gate,
    conv_taps,
    norm_input,
    norm_gain,
):
    groups = lax.axis_size(SP)
    ny, nx = lax.axis_size("ty"), lax.axis_size("tx")
    lane_count = ny * nx
    lane_index = lax.axis_index(TP)
    core = lax.axis_index("core").astype(i32).reshape(1)
    tok_rows, model_width = moe_input.shape
    top_count = route_ids.shape[1]
    capacity = tok_rows * top_count * 3 // (2 * groups)
    total = groups * capacity
    width = model_width // lane_count
    pitch = 40
    back_pitch = 24
    first_groups, second_groups = line_groups(ny, nx)
    channel_part = norm_input.shape[0]
    channels = channel_part * lane_count
    struct = jax.ShapeDtypeStruct

    own_block = pl.BlockSpec((tok_rows, width), lambda i, lane: (0, lane[0]))

    def fixed(*shape):
        return pl.BlockSpec(shape, lambda i, lane: (0,) * len(shape))

    sent, back_place, own_grad = pl.pallas_call(
        lambda *refs: prep_kernel(*refs, capacity=capacity, experts=groups),
        grid_spec=pltpu.PrefetchScalarGridSpec(
            num_scalar_prefetch=1,
            grid=(1,),
            in_specs=[fixed(top_count, tok_rows), fixed(top_count, tok_rows), own_block, own_block],
            out_specs=[fixed(groups * pitch, width), fixed(groups * back_pitch, tok_rows), fixed(tok_rows, width)],
        ),
        out_shape=[
            struct((groups * pitch, width), bf16),
            struct((groups * back_pitch, tok_rows), bf16),
            struct((tok_rows, width), bf16),
        ],
        compiler_params=params(16),
        name="prep",
    )(lane_index.astype(i32).reshape(1), route_ids.T, route_weights.T, moe_input, out_grad)

    part = exchanged(sent.reshape(groups, pitch, width), SP)

    gathered_rows = 2 * total + channel_part * 3 // 2
    spread = pl.pallas_call(
        lambda *refs: compact_kernel(*refs, capacity=capacity, pitch=pitch, sources=groups, group=8),
        out_shape=struct((nx, gathered_rows, width), bf16),
        in_specs=[whole(), whole()],
        out_specs=whole(),
        compiler_params=params(16),
        name="compact",
    )(part.reshape(groups * pitch, width), norm_input)
    line = exchanged(spread, PLANE, first_groups)
    gathered = exchanged(jnp.broadcast_to(line[None], (ny, *line.shape)), PLANE, second_groups)

    w_gate, w_up, w_down = expert_gate[0], expert_up[0], expert_down[0]
    ff = w_gate.shape[1]
    steps = 2
    chunk = total // steps

    def chunk_of(at):
        return pl.BlockSpec((ny, nx, chunk, width), lambda i, s: (0, 0, i + at, 0))

    input_grad, hidden, both = pl.pallas_call(
        expert_kernel,
        grid_spec=pltpu.PrefetchScalarGridSpec(
            num_scalar_prefetch=1,
            grid=(steps,),
            in_specs=[
                chunk_of(0),
                chunk_of(steps),
                fixed(model_width, ff),
                fixed(model_width, ff),
                fixed(ff, model_width),
            ],
            out_specs=[
                pl.BlockSpec((lane_count, chunk, width), lambda i, s: (0, i, 0)),
                pl.BlockSpec((chunk, ff), lambda i, s: (i, 0)),
                pl.BlockSpec((chunk, 2 * ff), lambda i, s: (i, 0)),
            ],
        ),
        out_shape=[
            struct((lane_count, total, width), bf16),
            struct((total, ff), bf16),
            struct((total, 2 * ff), bf16),
        ],
        compiler_params=params(36),
        cost_estimate=cost(10 * total * model_width * ff, 10 * total * model_width),
        name="expert",
    )(core, gathered, gathered, w_gate, w_up, w_down)

    summed_parts = exchanged(input_grad, TP)

    def piece_block(at):
        def index(j, s):
            y, x = j // nx, j % nx
            return (jnp.where(s[0] == 0, y, x), jnp.where(s[0] == 0, x, y), at, 0)

        return pl.BlockSpec((1, 1, total, width), index)

    gate_wgrad, up_wgrad, down_grad = pl.pallas_call(
        weight_kernel,
        grid_spec=pltpu.PrefetchScalarGridSpec(
            num_scalar_prefetch=1,
            grid=(lane_count,),
            in_specs=[piece_block(0), piece_block(1), fixed(total, ff), fixed(total, 2 * ff)],
            out_specs=[
                pl.BlockSpec((width, ff), lambda j, s: (j, 0)),
                pl.BlockSpec((width, ff), lambda j, s: (j, 0)),
                pl.BlockSpec((ff, width), lambda j, s: (0, j)),
            ],
        ),
        out_shape=[
            struct((model_width, ff), bf16),
            struct((model_width, ff), bf16),
            struct((ff, model_width), bf16),
        ],
        compiler_params=params(16),
        cost_estimate=cost(6 * total * model_width * ff, 10 * total * model_width),
        name="weights",
    )(core, gathered, gathered, hidden, both)

    norm_rows = channel_part * 3 // 2
    act, slope, cross, stats = pl.pallas_call(
        norm_kernel,
        grid_spec=pltpu.PrefetchScalarGridSpec(
            num_scalar_prefetch=1,
            grid=(1,),
            in_specs=[
                pl.BlockSpec((ny, nx, norm_rows, width), lambda i, s: (0, 0, 2 * total // norm_rows, 0)),
                fixed(channels, 1),
            ],
            out_specs=[
                fixed(channels, tok_rows),
                fixed(channels, tok_rows),
                fixed(channels, tok_rows),
                fixed(2, tok_rows),
            ],
        ),
        out_shape=[
            struct((channels, tok_rows), bf16),
            struct((channels, tok_rows), f32),
            struct((channels, tok_rows), f32),
            struct((2, tok_rows), f32),
        ],
        compiler_params=params(24),
        cost_estimate=cost(6 * total * model_width * ff, 10 * total * model_width),
        name="norm",
    )(core, gathered, norm_gain[:, None])

    summed_grad = pl.pallas_call(
        lambda *refs: row_sum_kernel(*refs, capacity=capacity, pitch=back_pitch, group=8),
        out_shape=struct((groups * back_pitch, width), bf16),
        in_specs=[whole()],
        out_specs=whole(),
        compiler_params=params(16),
        name="row_sum",
    )(summed_parts)
    returned = exchanged(summed_grad.reshape(groups, back_pitch, width), SP)

    proj_size = channels // groups
    block_rows = norm_rows + 8
    kept, given, blocks = pl.pallas_call(
        mix_kernel,
        out_shape=[
            struct((groups // 2, proj_size, width), f32),
            struct((groups // 2, proj_size, width), bf16),
            struct((lane_count, block_rows, width), bf16),
        ],
        in_specs=[scalar()] + [whole()] * 7,
        out_specs=[whole()] * 3,
        compiler_params=params(24),
        name="mix",
    )(
        core,
        back_place,
        returned.reshape(groups * back_pitch, width),
        own_grad,
        proj_weight,
        act,
        slope,
        cross,
    )
    arrived = exchanged(blocks, TP)
    from_pair = lax.ppermute(given, "core", [(0, 1), (1, 0)])
    chip_sum = (kept + from_pair.astype(f32)).astype(bf16)
    chip_sum, arrived = lax.optimization_barrier((chip_sum, arrived))
    grad_proj = jnp.sum(exchanged(chip_sum, "z").astype(f32), axis=0)

    taps_count = conv_taps.shape[1]
    reach_back = taps_count - 1
    gain_own = lax.dynamic_slice_in_dim(norm_gain, lane_index * channel_part, channel_part, 0)
    grad_conv, head = pl.pallas_call(
        lambda *refs: conv_grad_kernel(*refs, channels=channels),
        out_shape=[struct((channel_part, tok_rows), f32), struct((channel_part, reach_back), f32)],
        in_specs=[whole()] * 4,
        out_specs=[whole()] * 2,
        compiler_params=params(16),
        name="conv_grad",
    )(arrived, norm_input, gain_own[:, None], stats)

    pairs = [(i, i - 1) for i in range(1, groups)]
    ahead_rows = lax.ppermute(head, SP, pairs)
    extended = jnp.concatenate([grad_conv, ahead_rows], axis=1)
    grad_glu = jnp.zeros_like(grad_conv)
    for tap_index in range(taps_count):
        grad_glu = (
            grad_glu
            + conv_taps[:, tap_index : tap_index + 1]
            * extended[:, reach_back - tap_index : reach_back - tap_index + tok_rows]
        )
    sigmoid_gate = jax.nn.sigmoid(glu_gate.astype(f32))
    grad_value = (grad_glu * sigmoid_gate).astype(bf16)
    grad_glu_gate = (
        grad_glu * glu_value.astype(f32) * sigmoid_gate * (1.0 - sigmoid_gate)
    ).astype(bf16)
    return (gate_wgrad[None], up_wgrad[None], down_grad[None], grad_proj, grad_value, grad_glu_gate)


def solution(mesh):
    finer = Mesh(mesh.devices.reshape(mesh.shape["sp"] // 2, 2, 4, 4), ("z", "core", "ty", "tx"))
    return jax.shard_map(
        body,
        mesh=finer,
        in_specs=(
            P(SP, None),
            P(SP, None),
            P(SP, None),
            P(SP, None),
            P(SP, None, TP),
            P(SP, None, TP),
            P(SP, TP, None),
            P(None, TP),
            P(TP, SP),
            P(TP, SP),
            P(TP, None),
            P(TP, SP),
            P(),
        ),
        out_specs=(
            P(SP, None, TP),
            P(SP, None, TP),
            P(SP, TP, None),
            P(SP, TP),
            P(TP, SP),
            P(TP, SP),
        ),
        check_vma=False,
    )
```

time: 292 us -> 212 us (0.73)
  waiting for transfers between devices: 111 us -> 56.5 us
  blocking collectives: 56.9 us -> 88 us
  Pallas kernels: 0 us -> 22.3 us
  matrix products: 20 us -> 0 us
  starting transfers between devices: 44.1 us -> 25.9 us
  other arithmetic: 18.6 us -> 4.68 us
  between operations: 14.9 us -> 1.12 us
  local copies, waits for them, and re-layouts: 24.8 us -> 12 us
    all_gather x1 -> x0, waiting for transfers between devices: 64.7 us -> none  [sent_together_2(): lax.all_gather(both, axis, axis=dim, tiled=True)]
    all_to_all x1 -> x3, blocking collectives: 41.5 us -> 88 us  [exchanged(): lax.all_to_all(blocks, axis, 0, 0, axis_index_groups=index_groups, tiled=...]
    pallas_call x0 -> x8, Pallas kernels: none -> 22.3 us  [the longest x1 12.1 us: body(): pl.pallas_call(weight_kernel, grid_spec=pltpu.PrefetchScalarGridSpec(num_...]
    dot_general x13 -> x0, matrix products: 20 us -> none  [the longest x1 2.76 us: body(): lax.dot_general(grad_rows, w_down, (((1,), (1,)), ((), ())), preferred_el...]
    all_to_all x5 -> x4, starting transfers between devices: 38.7 us -> 19.5 us  [exchanged(): lax.all_to_all(blocks, axis, 0, 0, axis_index_groups=index_groups, tiled=...]
    psum x2 -> x0, blocking collectives: 15.4 us -> none  [over_axes(): shard = lax.psum(shard, axis)]
    all_to_all x5 -> x4, waiting for transfers between devices: 45.3 us -> 56.5 us  [exchanged(): lax.all_to_all(blocks, axis, 0, 0, axis_index_groups=index_groups, tiled=...]
    reshape x7 -> x0, local copies, waits for them, and re-layouts: 11.1 us -> none  [the longest x1 4.33 us: body(): grad_rows = arrived_grad.reshape(-1, model_width)]
  transfers between devices with their start and end apart: 7 -> 6, of which waited for: 5 -> 3; matrix products, arithmetic and copies ran while one was open for 16% -> 2% of each run, Pallas kernels for 0% -> 7%
where the time goes in v1:
time: 212 us; the launch traced here: 211 us
  blocking collectives  88 us (42%)
  waiting for transfers between devices  56.5 us (27%)
  starting transfers between devices  25.9 us (12%)
  Pallas kernels  22.3 us (11%)
  local copies, waits for them, and re-layouts  12 us (6%)
  other arithmetic  4.68 us (2%)
    all_to_all x3, blocking collectives, exchanged(): lax.all_to_all(blocks, axis, 0, 0, axis_index_groups=index_groups, tiled=...  88 us
    all_to_all x4, waiting for transfers between devices, exchanged(): lax.all_to_all(blocks, axis, 0, 0, axis_index_groups=index_groups, tiled=...  56.5 us
    all_to_all x4, starting transfers between devices, exchanged(): lax.all_to_all(blocks, axis, 0, 0, axis_index_groups=index_groups, tiled=...  19.5 us
    pallas_call x1, Pallas kernels, body(): pl.pallas_call(weight_kernel, grid_spec=pltpu.PrefetchScalarGridSpec(num_...  12.1 us
    unnamed x74, local copies, waits for them, and re-layouts  7.95 us
  transfers between devices with their start and end apart: 6, of which 3 were waited for; matrix products, arithmetic and copies ran while one was open for 2% of the time, Pallas kernels for 7%

profile of v1, /device:TPU:1, one launch (start us, length us, event | category | flops | bytes accessed | tf_op | source)
XLA Modules:
  0.0 210.5 jit_solution(14666577450401803186)
XLA Ops:
  0.6 1.1 copy-done
  1.8 1.1 copy-done.1
  2.9 0.7 copy-done.15
  3.6 0.7 copy-done.16
  4.3 0.9 prep.1
  5.2 0.0 copy-start.5
  5.2 41.5 %all_to_all.35 = bf16[32,40,128]{2,1,0:T(8,128)(2,1)S(1)} all-to-all(bf16[32,40,128]{2,1,0:T(8,128)(2,1)S(1)} %bitcast.84), channel_id=1, replica_groups=mesh['z'=16,'core'=2,'ty'=4,'tx'=4] {'z','core'}, dimensions={0} | all-to-all | bytes 655360 | tf_op jit(solution)/shard_map/all_to_all | solution.py:19
  46.8 0.8 copy-done.11
  47.5 0.5 compact.1
  48.0 15.3 %all_to_all.36 = bf16[4,1248,128]{2,1,0:T(8,128)(2,1)S(1)} all-to-all(bf16[4,1248,128]{2,1,0:T(8,128)(2,1)S(1)} %compact.1), channel_id=1, replica_groups={{0,1,2,3},{4,5,6,7},{8,9,10,11},{12,13,14,15},{16,20,24,28},{17,21,25,2..., dimensions={0} | all-to-all | bytes 2555904 | tf_op jit(solution)/shard_map/all_to_all | solution.py:19
  63.3 3.0 %broadcast_in_dim.21 = bf16[4,4,1248,128]{3,2,1,0:T(8,128)(2,1)} broadcast(bf16[4,1248,128]{2,1,0:T(8,128)(2,1)S(1)} %all_to_all.36), dimensions={1,2,3} | broadcast | bytes 6389760 | tf_op jit(solution)/shard_map/broadcast_in_dim | solution.py:343
  66.3 5.2 %all-to-all-start.2 = ((bf16[4,4,1248,128]{3,2,1,0:T(8,128)(2,1)}), bf16[4,4,1248,128]{3,2,1,0:T(8,128)(2,1)}, u32[]{:S(2)}, u32[]{:S(2)}) async-start(bf16[4,4,1248,128]{3,2,1,0:T(8,128)(2,1)} %broadcast_in_dim.21), calls=%async_computation.2 | async-start | bytes 10223616 | tf_op jit(solution)/shard_map/all_to_all | solution.py:19
  71.5 31.9 %all-to-all-done.2.rows_ref.grads_ref.parts_ref = bf16[4,4,1248,128]{3,2,1,0:T(8,128)(2,1)} async-done(((bf16[4,4,1248,128]{3,2,1,0:T(8,128)(2,1)}), bf16[4,4,1248,128]{3,2,1,0:T(8,128)(2,1)}, u32[]{:S(2)}, u32[]{:S(2)}) %all-to-all-start.2) | async-done | bytes 5111840 | tf_op jit(solution)/shard_map/all_to_all | solution.py:19
  103.3 4.2 %expert.1 = (bf16[16,576,128]{2,1,0:T(8,128)(2,1)S(1)}, bf16[576,128]{1,0:T(8,128)(2,1)S(1)}, bf16[576,256]{1,0:T(8,128)(2,1)S(1)}) custom-call(s32[1]{0:T(128)} %bitcast.core_ref, bf16[4,4,1248,128]{3,2,1,0:T(8,128)(2,1)} %all-to-all-done.2.rows_ref.grads_ref.parts_ref, bf16[4,4,1248,128]{3,2,1,0:T(8,128)(2,1)} %all-to-all-done.2.rows_ref.grads_ref.parts_ref, ...), custom_call_target="tpu_custom_call" | custom-call | flops 1509949440 | bytes 11796480 | tf_op jit(solution)/shard_map/expert/pallas_call | solution.py:353
  107.5 0.0 copy-start.7
  107.5 31.2 %all_to_all.37.refs_0_ = bf16[16,576,128]{2,1,0:T(8,128)(2,1)S(1)} all-to-all(bf16[16,576,128]{2,1,0:T(8,128)(2,1)S(1)} %get-tuple-element.33), channel_id=1, replica_groups=mesh['z'=16,'core'=2,'ty'=4,'tx'=4] {'ty','tx'}, dimensions={0} | all-to-all | bytes 4718592 | tf_op jit(solution)/shard_map/all_to_all | solution.py:19
  138.7 1.2 row_sum.1
  139.9 7.2 %all-to-all-start.4 = ((bf16[32,24,128]{2,1,0:T(8,128)(2,1)}), bf16[32,24,128]{2,1,0:T(8,128)(2,1)S(1)}, u32[]{:S(2)}, u32[]{:S(2)}) async-start(bf16[32,24,128]{2,1,0:T(8,128)(2,1)} %bitcast.12), calls=%async_computation.4 | async-start | bytes 393216 | tf_op jit(solution)/shard_map/all_to_all | solution.py:19
  147.2 0.0 copy-done.20
  147.2 0.2 copy.20.gain_ref
  147.4 0.1 dynamic-slice_bitcast_fusion
  147.5 0.1 copy.21.refs_2_
  147.6 0.6 slice_bitcast_fusion.30
  148.2 1.8 norm.1
  150.0 16.1 %all-to-all-done.4 = bf16[32,24,128]{2,1,0:T(8,128)(2,1)S(1)} async-done(((bf16[32,24,128]{2,1,0:T(8,128)(2,1)}), bf16[32,24,128]{2,1,0:T(8,128)(2,1)S(1)}, u32[]{:S(2)}, u32[]{:S(2)}) %all-to-all-start.4) | async-done | bytes 196640 | tf_op jit(solution)/shard_map/all_to_all | solution.py:19
  166.1 1.0 copy-done.6
  167.1 0.9 copy-done.10
  168.1 0.8 copy-done.14
  168.9 1.5 mix.1
  170.4 0.7 copy-done.9
  171.1 3.4 %collective-permute-start = (bf16[16,32,128]{2,1,0:T(8,128)(2,1)}, bf16[16,32,128]{2,1,0:T(8,128)(2,1)S(1)}, u32[]{:S(2)}, u32[]{:S(2)}) collective-permute-start(bf16[16,32,128]{2,1,0:T(8,128)(2,1)} %get-tuple-element.39), channel_id=1, source_target_pairs={{0,16},{16,0},{1,17},{17,1},{2,18},{18,2},{3,19},{19,3},{4,20},{20... | collective-permute-start | bytes 393224 | tf_op jit(solution)/shard_map/ppermute | solution.py:474
  174.5 3.6 %all-to-all-start.5 = ((bf16[16,104,128]{2,1,0:T(8,128)(2,1)}), bf16[16,104,128]{2,1,0:T(8,128)(2,1)S(1)}, u32[]{:S(2)}, u32[]{:S(2)}) async-start(bf16[16,104,128]{2,1,0:T(8,128)(2,1)} %get-tuple-element.40), calls=%async_computation.5 | async-start | bytes 851968 | tf_op jit(solution)/shard_map/all_to_all | solution.py:19
  178.1 0.0 collective-permute-done
  178.1 1.6 add_convert_fusion
  179.7 8.6 %all-to-all-done.5.refs_0_ = bf16[16,104,128]{2,1,0:T(8,128)(2,1)S(1)} async-done(((bf16[16,104,128]{2,1,0:T(8,128)(2,1)}), bf16[16,104,128]{2,1,0:T(8,128)(2,1)S(1)}, u32[]{:S(2)}, u32[]{:S(2)}) %all-to-all-start.5) | async-done | bytes 426016 | tf_op jit(solution)/shard_map/all_to_all | solution.py:19
  188.3 3.5 %all-to-all-start.6 = ((bf16[16,32,128]{2,1,0:T(8,128)(2,1)}), bf16[16,32,128]{2,1,0:T(8,128)(2,1)S(1)}, u32[]{:S(2)}, u32[]{:S(2)}) async-start(bf16[16,32,128]{2,1,0:T(8,128)(2,1)} %add_convert_fusion), calls=%async_computation.6 | async-start | bytes 262144 | tf_op jit(solution)/shard_map/all_to_all | solution.py:19
  191.8 0.1 conv_grad.1
  191.9 3.1 %collective-permute-start.1 = (f32[64,30]{1,0:T(8,128)S(1)}, f32[64,30]{1,0:T(8,128)S(1)}, u32[]{:S(2)}, u32[]{:S(2)}) collective-permute-start(f32[64,30]{1,0:T(8,128)S(1)} %get-tuple-element.45), channel_id=1, source_target_pairs={{16,0},{32,16},{48,32},{64,48},{80,64},{96,80},{112,96},{128,112},... | collective-permute-start | bytes 23048 | tf_op jit(solution)/shard_map/ppermute | solution.py:492
  195.0 0.0 copy-start.17
  195.0 0.0 copy-start.18
  195.0 0.0 copy-start.21
  195.1 0.0 copy-start.22
  195.2 12.1 %weights.1 = (bf16[2048,128]{1,0:T(8,128)(2,1)}, bf16[2048,128]{1,0:T(8,128)(2,1)}, bf16[128,2048]{1,0:T(8,128)(2,1)}) custom-call(s32[1]{0:T(128)} %bitcast.core_ref, bf16[4,4,1248,128]{3,2,1,0:T(8,128)(2,1)} %all-to-all-done.2.rows_ref.grads_ref.parts_ref, bf16[4,4,1248,128]{3,2,1,0:T(8,128)(2,1)} %all-to-all-done.2.rows_ref.grads_ref.parts_ref, ...), custom_call_target="tpu_custom_call" | custom-call | flops 905969664 | bytes 11796480 | tf_op jit(solution)/shard_map/weights/pallas_call | solution.py:390
  207.3 0.0 collective-permute-done.1
  207.5 1.8 multiply_convert_fusion
  209.3 0.6 multiply_convert_fusion.1
  209.9 0.0 all-to-all-done.6
  209.9 0.6 convert_reduce_fusion
  (59 shorter events, 0.1 us)
Async XLA Ops:
  0.6 1.1 copy-start
  1.8 1.1 copy-start.1
  2.9 0.7 copy-start.15
  3.6 0.7 copy-start.16
  5.2 41.5 %copy-start.5 = (bf16[768,192]{1,0:T(8,128)(2,1)}, bf16[768,192]{1,0:T(8,128)(2,1)S(1)}, u32[]{:S(2)}) copy-start(bf16[768,192]{1,0:T(8,128)(2,1)S(1)} %get-tuple-element.32.back_ref) | copy-start | bytes 884740
  5.2 42.8 %copy-start.13 = (bf16[192,128]{1,0:T(8,128)(2,1)}, bf16[192,128]{1,0:T(8,128)(2,1)S(1)}, u32[]{:S(2)}) copy-start(bf16[192,128]{1,0:T(8,128)(2,1)S(1)} %get-tuple-element.34.own_ref) | copy-start | bytes 147460
  46.8 0.8 copy-start.11
  66.3 37.1 %copy-start.2 = (bf16[1,2048,128]{2,1,0:T(8,128)(2,1)S(1)}, bf16[1,2048,128]{2,1,0:T(8,128)(2,1)}, u32[]{:S(2)}) copy-start(bf16[1,2048,128]{2,1,0:T(8,128)(2,1)} %param.17) | copy-start | bytes 1572868
  66.3 37.1 %copy-start.3 = (bf16[1,2048,128]{2,1,0:T(8,128)(2,1)S(1)}, bf16[1,2048,128]{2,1,0:T(8,128)(2,1)}, u32[]{:S(2)}) copy-start(bf16[1,2048,128]{2,1,0:T(8,128)(2,1)} %param.18) | copy-start | bytes 1572868
  66.3 37.1 %copy-start.4 = (bf16[1,128,2048]{2,1,0:T(8,128)(2,1)S(1)}, bf16[1,128,2048]{2,1,0:T(8,128)(2,1)}, u32[]{:S(2)}) copy-start(bf16[1,128,2048]{2,1,0:T(8,128)(2,1)} %param.19) | copy-start | bytes 1572868
  66.3 37.1 %all-to-all-start.2 = ((bf16[4,4,1248,128]{3,2,1,0:T(8,128)(2,1)}), bf16[4,4,1248,128]{3,2,1,0:T(8,128)(2,1)}, u32[]{:S(2)}, u32[]{:S(2)}) async-start(bf16[4,4,1248,128]{3,2,1,0:T(8,128)(2,1)} %broadcast_in_dim.21), calls=%async_computation.2 | async-start | bytes 10223616 | tf_op jit(solution)/shard_map/all_to_all | solution.py:19
  107.5 31.2 %copy-start.7 = (bf16[576,256]{1,0:T(8,128)(2,1)}, bf16[576,256]{1,0:T(8,128)(2,1)S(1)}, u32[]{:S(2)}) copy-start(bf16[576,256]{1,0:T(8,128)(2,1)S(1)} %get-tuple-element.28.both_ref) | copy-start | bytes 884740
  138.7 8.4 %copy-start.20 = (f32[1024]{0:T(1024)S(1)}, f32[1024]{0:T(1024)}, u32[]{:S(2)}) copy-start(f32[1024]{0:T(1024)} %param.25) | copy-start | bytes 12292
  138.7 8.9 %copy-start.19 = (f32[64,31]{0,1:T(8,128)S(1)}, f32[64,31]{0,1:T(8,128)}, u32[]{:S(2)}) copy-start(f32[64,31]{0,1:T(8,128)} %param.23) | copy-start | bytes 23812
  139.9 26.2 %all-to-all-start.4 = ((bf16[32,24,128]{2,1,0:T(8,128)(2,1)}), bf16[32,24,128]{2,1,0:T(8,128)(2,1)S(1)}, u32[]{:S(2)}, u32[]{:S(2)}) async-start(bf16[32,24,128]{2,1,0:T(8,128)(2,1)} %bitcast.12), calls=%async_computation.4 | async-start | bytes 393216 | tf_op jit(solution)/shard_map/all_to_all | solution.py:19
  166.1 1.0 copy-start.6
  167.1 0.9 copy-start.10
  168.1 0.8 copy-start.14
  168.9 22.9 %copy-start.12 = (bf16[64,192]{1,0:T(8,128)(2,1)S(1)}, bf16[64,192]{1,0:T(8,128)(2,1)}, u32[]{:S(2)}) copy-start(bf16[64,192]{1,0:T(8,128)(2,1)} %refs_1_.3) | copy-start | bytes 73732
  170.4 0.7 copy-start.9
  171.1 23.9 %copy-start.8 = (bf16[576,256]{1,0:T(8,128)(2,1)S(1)}, bf16[576,256]{1,0:T(8,128)(2,1)}, u32[]{:S(2)}) copy-start(bf16[576,256]{1,0:T(8,128)(2,1)} %copy-done.7) | copy-start | bytes 884740
  171.1 7.0 %collective-permute-start = (bf16[16,32,128]{2,1,0:T(8,128)(2,1)}, bf16[16,32,128]{2,1,0:T(8,128)(2,1)S(1)}, u32[]{:S(2)}, u32[]{:S(2)}) collective-permute-start(bf16[16,32,128]{2,1,0:T(8,128)(2,1)} %get-tuple-element.39), channel_id=1, source_target_pairs={{0,16},{16,0},{1,17},{17,1},{2,18},{18,2},{3,19},{19,3},{4,20},{20... | collective-permute-start | bytes 393224 | tf_op jit(solution)/shard_map/ppermute | solution.py:474
  174.5 13.8 %all-to-all-start.5 = ((bf16[16,104,128]{2,1,0:T(8,128)(2,1)}), bf16[16,104,128]{2,1,0:T(8,128)(2,1)S(1)}, u32[]{:S(2)}, u32[]{:S(2)}) async-start(bf16[16,104,128]{2,1,0:T(8,128)(2,1)} %get-tuple-element.40), calls=%async_computation.5 | async-start | bytes 851968 | tf_op jit(solution)/shard_map/all_to_all | solution.py:19
  188.3 21.6 %all-to-all-start.6 = ((bf16[16,32,128]{2,1,0:T(8,128)(2,1)}), bf16[16,32,128]{2,1,0:T(8,128)(2,1)S(1)}, u32[]{:S(2)}, u32[]{:S(2)}) async-start(bf16[16,32,128]{2,1,0:T(8,128)(2,1)} %add_convert_fusion), calls=%async_computation.6 | async-start | bytes 262144 | tf_op jit(solution)/shard_map/all_to_all | solution.py:19
  191.9 15.4 %collective-permute-start.1 = (f32[64,30]{1,0:T(8,128)S(1)}, f32[64,30]{1,0:T(8,128)S(1)}, u32[]{:S(2)}, u32[]{:S(2)}) collective-permute-start(f32[64,30]{1,0:T(8,128)S(1)} %get-tuple-element.45), channel_id=1, source_target_pairs={{16,0},{32,16},{48,32},{64,48},{80,64},{96,80},{112,96},{128,112},... | collective-permute-start | bytes 23048 | tf_op jit(solution)/shard_map/ppermute | solution.py:492
  195.0 12.3 %copy-start.17 = (bf16[64,192]{1,0:T(8,128)(2,1)S(1)}, bf16[64,192]{1,0:T(8,128)(2,1)}, u32[]{:S(2)}) copy-start(bf16[64,192]{1,0:T(8,128)(2,1)} %param.22) | copy-start | bytes 73732
  195.0 12.3 %copy-start.18 = (bf16[64,192]{1,0:T(8,128)(2,1)S(1)}, bf16[64,192]{1,0:T(8,128)(2,1)}, u32[]{:S(2)}) copy-start(bf16[64,192]{1,0:T(8,128)(2,1)} %param.21) | copy-start | bytes 73732
  195.0 12.3 %copy-start.21 = (f32[64]{0:T(128)S(1)}, f32[64]{0:T(128)}, u32[]{:S(2)}) copy-start(f32[64]{0:T(128)} %get-tuple-element.51) | copy-start | bytes 772
  195.1 12.3 %copy-start.22 = (f32[64]{0:T(128)S(1)}, f32[64]{0:T(128)}, u32[]{:S(2)}) copy-start(f32[64]{0:T(128)} %get-tuple-element.52) | copy-start | bytes 772
  195.1 12.3 %copy-start.23 = (f32[64]{0:T(128)S(1)}, f32[64]{0:T(128)}, u32[]{:S(2)}) copy-start(f32[64]{0:T(128)} %get-tuple-element.53) | copy-start | bytes 772
  195.1 12.3 %copy-start.24 = (f32[64]{0:T(128)S(1)}, f32[64]{0:T(128)}, u32[]{:S(2)}) copy-start(f32[64]{0:T(128)} %get-tuple-element.54) | copy-start | bytes 772
  195.1 12.3 %copy-start.25 = (f32[64]{0:T(128)S(1)}, f32[64]{0:T(128)}, u32[]{:S(2)}) copy-start(f32[64]{0:T(128)} %get-tuple-element.55) | copy-start | bytes 772
  195.1 12.3 %copy-start.26 = (f32[64]{0:T(128)S(1)}, f32[64]{0:T(128)}, u32[]{:S(2)}) copy-start(f32[64]{0:T(128)} %get-tuple-element.56) | copy-start | bytes 772
  195.1 12.3 %copy-start.27 = (f32[64]{0:T(128)S(1)}, f32[64]{0:T(128)}, u32[]{:S(2)}) copy-start(f32[64]{0:T(128)} %get-tuple-element.57) | copy-start | bytes 772
  195.1 12.3 %copy-start.28 = (f32[64]{0:T(128)S(1)}, f32[64]{0:T(128)}, u32[]{:S(2)}) copy-start(f32[64]{0:T(128)} %get-tuple-element.58) | copy-start | bytes 772
  195.1 12.3 %copy-start.29 = (f32[64]{0:T(128)S(1)}, f32[64]{0:T(128)}, u32[]{:S(2)}) copy-start(f32[64]{0:T(128)} %get-tuple-element.59) | copy-start | bytes 772
  195.1 12.3 %copy-start.30 = (f32[64]{0:T(128)S(1)}, f32[64]{0:T(128)}, u32[]{:S(2)}) copy-start(f32[64]{0:T(128)} %get-tuple-element.60) | copy-start | bytes 772
  195.1 12.3 %copy-start.31 = (f32[64]{0:T(128)S(1)}, f32[64]{0:T(128)}, u32[]{:S(2)}) copy-start(f32[64]{0:T(128)} %get-tuple-element.61) | copy-start | bytes 772
  195.2 12.3 %copy-start.32 = (f32[64]{0:T(128)S(1)}, f32[64]{0:T(128)}, u32[]{:S(2)}) copy-start(f32[64]{0:T(128)} %get-tuple-element.62) | copy-start | bytes 772
  195.2 12.3 %copy-start.33 = (f32[64]{0:T(128)S(1)}, f32[64]{0:T(128)}, u32[]{:S(2)}) copy-start(f32[64]{0:T(128)} %get-tuple-element.63) | copy-start | bytes 772
  195.2 12.3 %copy-start.34 = (f32[64]{0:T(128)S(1)}, f32[64]{0:T(128)}, u32[]{:S(2)}) copy-start(f32[64]{0:T(128)} %get-tuple-element.64) | copy-start | bytes 772
  195.2 12.3 %copy-start.35 = (f32[64]{0:T(128)S(1)}, f32[64]{0:T(128)}, u32[]{:S(2)}) copy-start(f32[64]{0:T(128)} %get-tuple-element.65) | copy-start | bytes 772
  195.2 12.3 %copy-start.36 = (f32[64]{0:T(128)S(1)}, f32[64]{0:T(128)}, u32[]{:S(2)}) copy-start(f32[64]{0:T(128)} %get-tuple-element.66) | copy-start | bytes 772
